TPU v7x, 256 devices: a whole 4x4x8 slice. The times are simulated.
256 devices in a mesh: ep: 64 (over z, y, core), tp: 4 (over x).
Axes of the slice: x: 4, y: 4, z: 8, core: 2. Of those that a mesh axis runs over, the one named last changes fastest.
Arguments:
- tokens: bfloat16 [1536, 2048], P('ep'), may hold values from -6 to 6
- norm_attn: float32 [2048], replicated, may hold values from 0.1 to 1.9
- w_query: bfloat16 [2048, 2048], P(None, 'tp'), may hold values from -0.125 to 0.125
- w_key: bfloat16 [2048, 256], P(None, 'tp'), may hold values from -0.125 to 0.125
- w_value: bfloat16 [2048, 256], P(None, 'tp'), may hold values from -0.125 to 0.125
- w_out: bfloat16 [2048, 2048], P('tp'), may hold values from -1 to 1
- head_bias: float32 [32], P('tp'), may hold values from -7 to -3
- key_cache: bfloat16 [1536, 4, 1024, 64], P('ep', 'tp'), may hold values from -6 to 6
- value_cache: bfloat16 [1536, 4, 1024, 64], P('ep', 'tp'), may hold values from -6 to 6
- lengths: int32 [1536], P('ep'), may hold values from 1 to 1024, 786432 in all
- norm_ffn: float32 [2048], replicated, may hold values from 0.1 to 1.9
- w_group: bfloat16 [2048, 4], replicated, may hold values from -0.125 to 0.125
- w_fine: bfloat16 [2048, 64], replicated, may hold values from -0.125 to 0.125
- routes: int32 [1536, 2], P('ep'), may hold values from 0 to 63, as said below
- e_gate: bfloat16 [64, 2048, 512], P('ep', 'tp'), may hold values from -0.125 to 0.125
- e_up: bfloat16 [64, 2048, 512], P('ep', 'tp'), may hold values from -0.125 to 0.125
- e_down: bfloat16 [64, 512, 2048], P('ep', None, 'tp'), may hold values from -1 to 1
- d_gate: bfloat16 [2048, 8192], P('tp', 'ep'), may hold values from -0.125 to 0.125
- d_up: bfloat16 [2048, 8192], P('tp', 'ep'), may hold values from -0.125 to 0.125
- d_down: bfloat16 [8192, 2048], P('ep', 'tp'), may hold values from -0.25 to 0.25
- w_mix: float32 [2048], replicated, may hold values from -0.125 to 0.125
Outputs:
- mixed: bfloat16 [1536, 2048], P('ep', 'tp')
- new_keys: bfloat16 [1536, 4, 64], P('ep', 'tp')
- new_values: bfloat16 [1536, 4, 64], P('ep', 'tp')
Inputs may be any that keep to these rules, and one draw needn't show every extreme that they name: `routes`: the 2 experts of a row are distinct and lie in one group of 16 consecutive experts. Among the rows of one device each expert is named at most 2 times. One group, the same on every device, is named by exactly 16 rows of every device, so that each of its experts is named exactly 2 times by every device.
All inputs are finite; a program needn't handle non-finite values. No bound on the sum of `lengths` on one device may be relied on, other than what follows from the above.
Results may differ from a plain program's by a relative error of at most 0.019.
Values may be sent and summed in bfloat16 or wider, within the bound.
No kernel may reach another device: no remote copies, remote signals or barrier semaphores. Data moves between devices by JAX's collectives and lax.ppermute only.
A program may use at most 128 MiB of HBM per device.

v0:
```python
import jax
import jax.numpy as jnp
from jax import lax
from jax.sharding import Mesh
from jax.sharding import PartitionSpec as P

GROUPS = 4
TOP_K = 2
EP = ("ep_0", "ep_1", "ep_2")
norm_eps = 1e-06
segment_len = 128


def copy_for_each(x, axis):
    devices = lax.axis_size(axis)
    return lax.all_to_all(jnp.broadcast_to(x[None], (devices, *x.shape)), axis, 0, 0, tiled=True)


def over_copies(x, axis):
    everything = copy_for_each(x, axis)
    return jnp.sum(everything.astype(jnp.float32), axis=0)


def in_order(tiles, dim):
    lengths = list(tiles.shape[1:])
    lengths[dim] *= tiles.shape[0]
    return jnp.moveaxis(tiles, 0, dim).reshape(lengths)


def all_blocks(x, axes, sequence):
    tiles = x[None]
    for k in sequence:
        tiles = lax.all_gather(tiles, axes[k], axis=0, tiled=True)
    current = [lax.axis_size(axes[k]) for k in reversed(sequence)]
    tiles = tiles.reshape(*current, *x.shape)
    turned = sorted(range(len(sequence)), key=lambda place: sequence[len(sequence) - 1 - place])
    return tiles.transpose(*turned, *range(len(sequence), tiles.ndim)).reshape(-1, *x.shape)


def whole_of(x, axes, sequence, dim):
    return in_order(all_blocks(x, axes, sequence), dim)


def normed(values, gains):
    wide = values.astype(jnp.float32)
    return wide * lax.rsqrt(jnp.mean(wide * wide, axis=-1, keepdims=True) + norm_eps) * gains


def suffix_sums(terms):
    length = terms.shape[-1]
    pieces = length // segment_len
    shaped = terms.reshape(terms.shape[:-1] + (pieces, segment_len))
    inner = lax.iota(jnp.int32, segment_len)
    later_inner = (inner[:, None] > inner[None, :]).astype(jnp.float32)
    within = jnp.einsum("...ij,jk->...ik", shaped, later_inner, precision=lax.Precision.HIGHEST)
    outer = lax.iota(jnp.int32, pieces)
    later_outer = (outer[:, None] > outer[None, :]).astype(jnp.float32)
    carried = jnp.einsum(
        "...i,ij->...j", jnp.sum(shaped, axis=-1), later_outer, precision=lax.Precision.HIGHEST
    )
    return (within + carried[..., None]).reshape(terms.shape)


def stick_read(queries, keys, values, lengths, bias_table):
    scores = jnp.einsum("bkgd,bksd->bkgs", queries, keys, preferred_element_type=jnp.float32)
    scores = scores * queries.shape[-1] ** (-0.5) + bias_table[None, :, :, None]
    positions = lax.iota(jnp.int32, keys.shape[2])
    inside = (positions[None, :] < lengths[:, None])[:, None, None, :]
    fails = jnp.where(inside, jax.nn.log_sigmoid(-scores), 0.0)
    weights = jnp.where(inside, jnp.exp(jax.nn.log_sigmoid(scores) + suffix_sums(fails)), 0.0)
    result = jnp.einsum(
        "bkgs,bksd->bkgd", weights.astype(jnp.bfloat16), values, preferred_element_type=jnp.float32
    )
    return result.astype(jnp.bfloat16).reshape(queries.shape[0], -1)


def route_weights(group_logits, fine_logits, chosen, per_group):
    group_iota = lax.iota(jnp.int32, group_logits.shape[1])
    own_group = chosen[:, 0] // per_group
    own_logit = jnp.sum(
        jnp.where(group_iota[None, :] == own_group[:, None], group_logits, 0.0), axis=1
    )
    group_share = 1.0 / jnp.sum(jnp.exp(group_logits - own_logit[:, None]), axis=1)
    expert_iota = lax.iota(jnp.int32, fine_logits.shape[1])
    picked = jnp.sum(
        jnp.where(expert_iota[None, None, :] == chosen[:, :, None], fine_logits[:, None, :], 0.0),
        axis=2,
    )
    within = 1.0 / jnp.sum(jnp.exp(picked[:, None, :] - picked[:, :, None]), axis=2)
    return group_share[:, None] * within


def slot_ranks(flat_routes):
    count = flat_routes.shape[0]
    same_expert = flat_routes[:, None] == flat_routes[None, :]
    position = lax.iota(jnp.int32, count)
    earlier = position[None, :] < position[:, None]
    return jnp.sum(same_expert & earlier, axis=1)


def shards(
    tokens,
    norm_attn,
    w_query,
    w_key,
    w_value,
    w_out,
    head_bias,
    key_cache,
    value_cache,
    lengths,
    norm_ffn,
    w_group,
    w_fine,
    routes,
    e_gate,
    e_up,
    e_down,
    d_gate,
    d_up,
    d_down,
    w_mix,
):
    seq_count = tokens.shape[0]
    width_part = d_gate.shape[0]
    dense_units = d_gate.shape[1]
    expert_units = e_gate.shape[2]
    kv_local = key_cache.shape[1]
    head_dim = key_cache.shape[3]
    ep_size = lax.axis_size(EP)
    per_group = ep_size // GROUPS
    capacity = max(2, (seq_count + per_group - 1) // per_group)
    h_first = normed(tokens, norm_attn).astype(jnp.bfloat16)
    queries = jnp.dot(h_first, w_query, preferred_element_type=jnp.float32).astype(jnp.bfloat16)
    new_keys = jnp.dot(h_first, w_key, preferred_element_type=jnp.float32).astype(jnp.bfloat16)
    new_values = jnp.dot(h_first, w_value, preferred_element_type=jnp.float32).astype(jnp.bfloat16)
    grouped = queries.reshape(seq_count, kv_local, -1, head_dim)
    heads_out = stick_read(
        grouped, key_cache, value_cache, lengths, head_bias.reshape(kv_local, -1)
    )
    partial_value = jnp.dot(heads_out, w_out, preferred_element_type=jnp.float32).astype(
        jnp.bfloat16
    )
    attended = over_copies(
        lax.optimization_barrier(partial_value).astype(jnp.float32).astype(jnp.bfloat16), "tp"
    ).astype(jnp.float32)
    resid = tokens.astype(jnp.float32) + attended
    h_second = normed(resid, norm_ffn).astype(jnp.bfloat16)
    column = lax.axis_index("tp") * width_part
    h_slice = lax.dynamic_slice_in_dim(h_second, column, width_part, 1)
    resid_slice = lax.dynamic_slice_in_dim(resid, column, width_part, 1)
    dense_in = jnp.concatenate([d_gate, d_up], axis=1)
    expert_in = jnp.concatenate([e_gate[0], e_up[0]], axis=1)
    group_logits = jnp.dot(h_second, w_group, preferred_element_type=jnp.float32)
    fine_logits = jnp.dot(h_second, w_fine, preferred_element_type=jnp.float32)
    shares = route_weights(group_logits, fine_logits, routes, per_group)
    mix_gate = jax.nn.sigmoid(
        jnp.dot(h_second.astype(jnp.float32), w_mix, precision=lax.Precision.HIGHEST)
    )
    flat_routes = routes.reshape(-1)
    slot_ids = flat_routes * capacity + slot_ranks(flat_routes)
    onehot = (lax.iota(jnp.int32, ep_size * capacity)[:, None] == slot_ids[None, :]).astype(
        jnp.float32
    )
    repeated = jnp.repeat(h_slice, TOP_K, axis=0)
    outbound = jnp.dot(onehot.astype(jnp.bfloat16), repeated, preferred_element_type=jnp.float32)
    outbound = outbound.astype(jnp.bfloat16).reshape(ep_size, capacity, width_part)
    received = lax.all_to_all(outbound, EP, split_axis=0, concat_axis=0, tiled=True)
    flat_rows = received.reshape(-1, width_part)
    pre_act = over_copies(
        jnp.dot(flat_rows, expert_in, preferred_element_type=jnp.float32).astype(jnp.bfloat16), "tp"
    ).astype(jnp.float32)
    hidden = (jax.nn.silu(pre_act[:, :expert_units]) * pre_act[:, expert_units:]).astype(
        jnp.bfloat16
    )
    result = jnp.dot(hidden, e_down[0], preferred_element_type=jnp.float32).astype(jnp.bfloat16)
    returned = lax.all_to_all(
        result.reshape(received.shape), EP, split_axis=0, concat_axis=0, tiled=True
    )
    weighted = onehot * shares.reshape(-1)[None, :]
    moe_rows = jnp.dot(
        weighted.T,
        returned.reshape(-1, width_part).astype(jnp.float32),
        precision=lax.Precision.HIGHEST,
    )
    moe_slice = jnp.sum(moe_rows.reshape(seq_count, TOP_K, width_part), axis=1)
    dense_pre = jnp.dot(
        whole_of(h_slice, EP, (1, 0, 2), 0), dense_in, preferred_element_type=jnp.float32
    )
    dense_pre = over_copies(dense_pre.astype(jnp.bfloat16), "tp").astype(jnp.float32)
    dense_hidden = (jax.nn.silu(dense_pre[:, :dense_units]) * dense_pre[:, dense_units:]).astype(
        jnp.bfloat16
    )
    own_hidden = lax.all_to_all(dense_hidden, EP, split_axis=0, concat_axis=1, tiled=True)
    dense_slice = jnp.dot(
        own_hidden,
        lax.all_gather(d_down, EP, axis=0, tiled=True),
        preferred_element_type=jnp.float32,
    )
    mixed = resid_slice + moe_slice + mix_gate[:, None] * dense_slice
    return (
        mixed.astype(jnp.bfloat16),
        new_keys.reshape(seq_count, kv_local, head_dim),
        new_values.reshape(seq_count, kv_local, head_dim),
    )


def solution(mesh):
    torus = Mesh(mesh.devices.reshape(8, 4, 2, mesh.shape["tp"]), ("ep_0", "ep_1", "ep_2", "tp"))
    placed = (
        P(EP, None),
        P(),
        P(None, "tp"),
        P(None, "tp"),
        P(None, "tp"),
        P("tp", None),
        P("tp"),
        P(EP, "tp", None, None),
        P(EP, "tp", None, None),
        P(EP),
        P(),
        P(),
        P(),
        P(EP, None),
        P(EP, "tp", None),
        P(EP, "tp", None),
        P(EP, None, "tp"),
        P("tp", EP),
        P("tp", EP),
        P(EP, "tp"),
        P(),
    )
    return jax.shard_map(
        shards,
        mesh=torus,
        in_specs=placed,
        out_specs=(P(EP, "tp"), P(EP, "tp", None), P(EP, "tp", None)),
        check_vma=False,
    )
```

profile of v0, /device:TPU:1, one launch (start us, length us, event | category | flops | bytes accessed | tf_op | source)
XLA Modules:
  0.0 220.9 jit_solution(17859736883952036732)
XLA Ops:
  7.2 1.2 fusion.44
  8.4 2.1 convolution_convert_fusion.5
  12.1 1.4 fusion.70
  13.9 2.6 %convolution_add_fusion = f32[24,8,8,128]{3,2,1,0:T(8,128)} fusion(f32[24,8,8,128]{3,1,2,0:T(8,128)} %get-tuple-element.6, f32[24,8,8]{2,1,0:T(8,128)S(1)} %copy.68), kind=kOutput, calls=%fused_computation.10 | convolution fusion | flops 302202880 | bytes 1579008 | tf_op jit(solution)/shard_map/...ij,jk->...ik/dot_general | solution.py:55
  16.5 2.1 reshape.207
  18.7 3.3 %fusion.10 = bf16[24,8,64]{2,1,0:T(8,128)(2,1)S(1)} fusion(bf16[24,1,1024,64]{2,3,1,0:T(8,128)(2,1)} %param.29, f32[24,8,1024]{2,1,0:T(8,128)} %reshape.207, f32[24,8,1024]{2,1,0:T(8,128)} %copy-done.1, pred[24,1024]{1,0:T(8,128)(4,1)S(1)} %iota_compare_fusion), kind=kOutput, calls=%fused_computation.16 | convolution fusion | flops 27340800 | bytes 4767744 | tf_op jit(solution)/shard_map/bkgs,bksd->bkgd/dot_general | solution.py:71
  22.1 2.0 convolution_convert_fusion.1
  24.9 5.0 %all-to-all-start = ((bf16[4,24,2048]{2,1,0:T(8,128)(2,1)}), bf16[4,24,2048]{2,1,0:T(8,128)(2,1)S(1)}, u32[]{:S(2)}, u32[]{:S(2)}) async-start(bf16[4,24,2048]{2,1,0:T(8,128)(2,1)} %broadcast_in_dim.41), calls=%async_computation | async-start | bytes 786432 | tf_op jit(solution)/shard_map/all_to_all | solution.py:16
  29.8 6.2 %all-to-all-done = bf16[4,24,2048]{2,1,0:T(8,128)(2,1)S(1)} async-done(((bf16[4,24,2048]{2,1,0:T(8,128)(2,1)}), bf16[4,24,2048]{2,1,0:T(8,128)(2,1)S(1)}, u32[]{:S(2)}, u32[]{:S(2)}) %all-to-all-start) | async-done | bytes 393248 | tf_op jit(solution)/shard_map/all_to_all | solution.py:16
  38.0 10.2 %all-gather = bf16[96,512]{1,0:T(8,128)(2,1)S(1)} all-gather(bf16[24,512]{1,0:T(8,128)(2,1)S(1)} %constant_dynamic-slice_fusion), channel_id=2, replica_groups=mesh['ep_0'=8,'ep_1'=4,'ep_2'=2,'tp'=4] {'ep_1'}, dimensions={0}, use_global_device_ids=true | all-gather | bytes 122880 | tf_op jit(solution)/shard_map/all_gather | solution.py:33
  48.2 26.3 %all_gather.13 = bf16[32,24,512]{2,1,0:T(8,128)(2,1)} all-gather(bf16[4,24,512]{2,1,0:T(8,128)(2,1)S(1)} %bitcast.85), channel_id=1, replica_groups=mesh['ep_0'=8,'ep_1'=4,'ep_2'=2,'tp'=4] {'ep_0'}, dimensions={0}, use_global_device_ids=true | all-gather | bytes 884736 | tf_op jit(solution)/shard_map/all_gather | solution.py:33
  76.0 28.8 %all_to_all.44 = bf16[64,2,512]{2,1,0:T(2,128)(2,1)S(1)} all-to-all(bf16[64,2,512]{2,1,0:T(2,128)(2,1)S(1)} %reshape.212), channel_id=1, replica_groups=mesh['ep_0'=8,'ep_1'=4,'ep_2'=2,'tp'=4] {'ep_0','ep_1','ep_2'}, dimensions={0} | all-to-all | bytes 262144 | tf_op jit(solution)/shard_map/all_to_all | solution.py:168
  104.8 1.5 convolution_convert_fusion.2
  106.4 1.1 broadcast_in_dim.46
  107.5 4.2 %all-to-all-start.2 = ((bf16[4,128,1024]{2,1,0:T(8,128)(2,1)}), bf16[4,128,1024]{2,1,0:T(8,128)(2,1)}, u32[]{:S(2)}, u32[]{:S(2)}) async-start(bf16[4,128,1024]{2,1,0:T(8,128)(2,1)} %broadcast_in_dim.46), calls=%async_computation.2 | async-start | bytes 2097152 | tf_op jit(solution)/shard_map/all_to_all | solution.py:16
  111.8 1.7 copy.71
  113.5 1.5 convolution_convert_fusion
  115.0 11.6 %all-to-all-done.2 = bf16[4,128,1024]{2,1,0:T(8,128)(2,1)} async-done(((bf16[4,128,1024]{2,1,0:T(8,128)(2,1)}), bf16[4,128,1024]{2,1,0:T(8,128)(2,1)}, u32[]{:S(2)}, u32[]{:S(2)}) %all-to-all-start.2) | async-done | bytes 1048608 | tf_op jit(solution)/shard_map/all_to_all | solution.py:16
  126.6 3.1 %broadcast_in_dim.48 = bf16[4,1536,256]{2,1,0:T(8,128)(2,1)} broadcast(bf16[1536,256]{1,0:T(8,128)(2,1)} %convolution_convert_fusion), dimensions={1,2} | broadcast | bytes 3932160 | tf_op jit(solution)/shard_map/broadcast_in_dim | solution.py:16
  129.7 4.8 %all-to-all-start.4 = ((bf16[4,1536,256]{2,1,0:T(8,128)(2,1)}), bf16[4,1536,256]{2,1,0:T(8,128)(2,1)}, u32[]{:S(2)}, u32[]{:S(2)}) async-start(bf16[4,1536,256]{2,1,0:T(8,128)(2,1)} %broadcast_in_dim.48), calls=%async_computation.4 | async-start | bytes 6291456 | tf_op jit(solution)/shard_map/all_to_all | solution.py:16
  134.7 1.9 fusion.15
  136.5 1.8 fusion.16
  139.9 1.5 convert_reduce_fusion.1
  142.3 28.6 %all-to-all-done.4 = bf16[4,1536,256]{2,1,0:T(8,128)(2,1)} async-done(((bf16[4,1536,256]{2,1,0:T(8,128)(2,1)}), bf16[4,1536,256]{2,1,0:T(8,128)(2,1)}, u32[]{:S(2)}, u32[]{:S(2)}) %all-to-all-start.4) | async-done | bytes 3145760 | tf_op jit(solution)/shard_map/all_to_all | solution.py:16
  171.0 6.1 %all-to-all-start.3 = ((bf16[64,2,512]{2,1,0:T(2,128)(2,1)}), bf16[64,2,512]{2,1,0:T(2,128)(2,1)S(1)}, u32[]{:S(2)}, u32[]{:S(2)}) async-start(bf16[64,2,512]{2,1,0:T(2,128)(2,1)} %reshape.214), calls=%async_computation.3 | async-start | bytes 262144 | tf_op jit(solution)/shard_map/all_to_all | solution.py:177
  177.1 2.6 %convert_reduce_fusion = f32[1536,256]{1,0:T(8,128)S(1)} fusion(bf16[4,1536,256]{2,1,0:T(8,128)(2,1)} %all-to-all-done.4), kind=kLoop, calls=%fused_computation | loop fusion | flops 2752512 | bytes 4718592 | tf_op jit(solution)/shard_map/reduce_sum | solution.py:21
  180.8 7.6 %all-to-all-done.3 = bf16[64,2,512]{2,1,0:T(2,128)(2,1)S(1)} async-done(((bf16[64,2,512]{2,1,0:T(2,128)(2,1)}), bf16[64,2,512]{2,1,0:T(2,128)(2,1)S(1)}, u32[]{:S(2)}, u32[]{:S(2)}) %all-to-all-start.3) | async-done | bytes 131104 | tf_op jit(solution)/shard_map/all_to_all | solution.py:177
  189.0 4.5 %all-to-all-start.5 = ((bf16[64,24,128]{2,1,0:T(8,128)(2,1)}), bf16[64,24,128]{2,1,0:T(8,128)(2,1)S(1)}, u32[]{:S(2)}, u32[]{:S(2)}) async-start(bf16[64,24,128]{2,1,0:T(8,128)(2,1)} %bitcast.84), calls=%async_computation.5 | async-start | bytes 786432 | tf_op jit(solution)/shard_map/all_to_all | solution.py:194
  194.5 1.7 reshape.222
  196.2 1.8 convolution_reduce_fusion
  198.0 10.8 %all-to-all-done.5 = bf16[64,24,128]{2,1,0:T(8,128)(2,1)S(1)} async-done(((bf16[64,24,128]{2,1,0:T(8,128)(2,1)}), bf16[64,24,128]{2,1,0:T(8,128)(2,1)S(1)}, u32[]{:S(2)}, u32[]{:S(2)}) %all-to-all-start.5) | async-done | bytes 393248 | tf_op jit(solution)/shard_map/all_to_all | solution.py:194
  208.8 5.3 %fusion.14 = bf16[24,512]{1,0:T(8,128)(2,1)} fusion(bf16[8192,512]{1,0:T(8,128)(2,1)} %all-gather.6.cloned.1.call-done, f32[24,512]{1,0:T(8,128)} %convolution_reduce_fusion, f32[24,2048]{1,0:T(8,128)} %copy-done.2, s32[]{:T(128)S(6)} %select_n.41, f32[24]{0:T(128)S(1)} %fusion.20, bf16[64,24,128]{2,1,0:T(8,128)(2,1)S(1)} %all-to-all-done.5), kind=kOutput, calls=%fused_computation.20 | convolution fusion | flops 201375744 | bytes 8904804 | tf_op jit(solution)/shard_map/dot_general | solution.py:195
  (74 shorter events, 11.5 us)
Async XLA Ops:
  7.2 3.5 %copy-start = (bf16[24,1,1024,64]{2,3,1,0:T(8,128)(2,1)S(1)}, bf16[24,1,1024,64]{2,3,1,0:T(8,128)(2,1)}, u32[]{:S(2)}) copy-start(bf16[24,1,1024,64]{2,3,1,0:T(8,128)(2,1)} %param.28) | copy-start | bytes 9437188
  7.2 3.4 %copy-start.10 = (s32[24]{0:T(128)S(1)}, s32[24]{0:T(128)}, u32[]{:S(2)}) copy-start(s32[24]{0:T(128)} %param.30) | copy-start | bytes 292
  7.2 3.5 %copy-start.9 = (f32[8]{0:T(128)S(1)}, f32[8]{0:T(128)}, u32[]{:S(2)}) copy-start(f32[8]{0:T(128)} %param.27) | copy-start | bytes 100
  11.2 0.9 copy-start.1
  22.1 15.8 %copy-start.8 = (f32[2048]{0:T(1024)S(1)}, f32[2048]{0:T(1024)}, u32[]{:S(2)}) copy-start(f32[2048]{0:T(1024)} %param.31) | copy-start | bytes 24580
  24.9 50.4 %copy-start.6 = (s32[24,2]{0,1:T(2,128)S(1)}, s32[24,2]{0,1:T(2,128)}, u32[]{:S(2)}) copy-start(s32[24,2]{0,1:T(2,128)} %param.34) | copy-start | bytes 580
  24.9 11.2 %all-to-all-start = ((bf16[4,24,2048]{2,1,0:T(8,128)(2,1)}), bf16[4,24,2048]{2,1,0:T(8,128)(2,1)S(1)}, u32[]{:S(2)}, u32[]{:S(2)}) async-start(bf16[4,24,2048]{2,1,0:T(8,128)(2,1)} %broadcast_in_dim.41), calls=%async_computation | async-start | bytes 786432 | tf_op jit(solution)/shard_map/all_to_all | solution.py:16
  29.8 82.0 %all-gather.4.cloned.1.call-start = ((), (), s32[]{:S(2)}) async-start(), calls=%async_computation.6 | async-start | bytes 2359296 | tf_op jit(solution)/shard_map/all_gather | solution.py:33
  37.2 0.7 copy-start.2
  37.9 100.6 %copy-start.5 = (bf16[24,2048]{1,0:T(8,128)(2,1)}, bf16[24,2048]{1,0:T(8,128)(2,1)S(1)}, u32[]{:S(2)}) copy-start(bf16[24,2048]{1,0:T(8,128)(2,1)S(1)} %multiply_convert_fusion) | copy-start | bytes 294916
  74.5 134.3 %all-gather.6.cloned.1.call-start = ((), (), s32[]{:S(2)}) async-start(), calls=%async_computation.7 | async-start | bytes 8519680 | tf_op jit(solution)/shard_map/all_gather | solution.py:197
  107.5 19.1 %all-to-all-start.2 = ((bf16[4,128,1024]{2,1,0:T(8,128)(2,1)}), bf16[4,128,1024]{2,1,0:T(8,128)(2,1)}, u32[]{:S(2)}, u32[]{:S(2)}) async-start(bf16[4,128,1024]{2,1,0:T(8,128)(2,1)} %broadcast_in_dim.46), calls=%async_computation.2 | async-start | bytes 2097152 | tf_op jit(solution)/shard_map/all_to_all | solution.py:16
  111.8 1.8 copy-start.12
  111.8 1.8 copy-start.13
  129.7 5.0 %copy-start.3 = (bf16[24,2048]{1,0:T(8,128)(2,1)S(1)}, bf16[24,2048]{1,0:T(8,128)(2,1)}, u32[]{:S(2)}) copy-start(bf16[24,2048]{1,0:T(8,128)(2,1)} %param.21) | copy-start | bytes 294916
  129.7 5.0 %copy-start.7 = (f32[2048]{0:T(1024)S(1)}, f32[2048]{0:T(1024)}, u32[]{:S(2)}) copy-start(f32[2048]{0:T(1024)} %param.22) | copy-start | bytes 24580
  129.7 8.7 %copy-start.14 = (bf16[2048,4]{0,1:T(4,128)(2,1)S(1)}, bf16[2048,4]{0,1:T(4,128)(2,1)}, u32[]{:S(2)}) copy-start(bf16[2048,4]{0,1:T(4,128)(2,1)} %param.32) | copy-start | bytes 49156
  129.7 41.3 %all-to-all-start.4 = ((bf16[4,1536,256]{2,1,0:T(8,128)(2,1)}), bf16[4,1536,256]{2,1,0:T(8,128)(2,1)}, u32[]{:S(2)}, u32[]{:S(2)}) async-start(bf16[4,1536,256]{2,1,0:T(8,128)(2,1)} %broadcast_in_dim.48), calls=%async_computation.4 | async-start | bytes 6291456 | tf_op jit(solution)/shard_map/all_to_all | solution.py:16
  134.7 6.7 %copy-start.11 = (bf16[1,512,512]{2,1,0:T(8,128)(2,1)S(1)}, bf16[1,512,512]{2,1,0:T(8,128)(2,1)}, u32[]{:S(2)}) copy-start(bf16[1,512,512]{2,1,0:T(8,128)(2,1)} %param.37) | copy-start | bytes 1572868
  171.0 17.4 %all-to-all-start.3 = ((bf16[64,2,512]{2,1,0:T(2,128)(2,1)}), bf16[64,2,512]{2,1,0:T(2,128)(2,1)S(1)}, u32[]{:S(2)}, u32[]{:S(2)}) async-start(bf16[64,2,512]{2,1,0:T(2,128)(2,1)} %reshape.214), calls=%async_computation.3 | async-start | bytes 262144 | tf_op jit(solution)/shard_map/all_to_all | solution.py:177
  188.4 0.6 copy-start.4
  189.0 19.8 %all-to-all-start.5 = ((bf16[64,24,128]{2,1,0:T(8,128)(2,1)}), bf16[64,24,128]{2,1,0:T(8,128)(2,1)S(1)}, u32[]{:S(2)}, u32[]{:S(2)}) async-start(bf16[64,24,128]{2,1,0:T(8,128)(2,1)} %bitcast.84), calls=%async_computation.5 | async-start | bytes 786432 | tf_op jit(solution)/shard_map/all_to_all | solution.py:194
Sparse Core Ops, SparseCore 0:
  74.7 22.5 all-gather.3
  100.0 85.2 all-gather.5
where the time goes:
time: 222 us; the launch traced here: 221 us
  waiting for transfers between devices  65.6 us (30%)
  blocking collectives  65.4 us (29%)
  matrix products  27.1 us (12%)
  starting transfers between devices  24.6 us (11%)
  local copies, waits for them, and re-layouts  14.4 us (6%)
  between operations  14.4 us (6%)
  other arithmetic  9.43 us (4%)
    all_to_all x3, waiting for transfers between devices, copy_for_each(): lax.all_to_all(jnp.broadcast_to(x[None], (devices, *x.shape)), axis, 0, 0...  46.5 us
    all_gather x2, blocking collectives, all_blocks(): tiles = lax.all_gather(tiles, axes[k], axis=0, tiled=True)  36.5 us
    all_to_all x1, blocking collectives, shards(): lax.all_to_all(outbound, EP, split_axis=0, concat_axis=0, tiled=True)  28.8 us
    all_to_all x3, starting transfers between devices, copy_for_each(): lax.all_to_all(jnp.broadcast_to(x[None], (devices, *x.shape)), axis, 0, 0...  14 us
    all_to_all x1, waiting for transfers between devices, shards(): lax.all_to_all(dense_hidden, EP, split_axis=0, concat_axis=1, tiled=True)  10.8 us
    all_to_all x1, waiting for transfers between devices, shards(): lax.all_to_all(result.reshape(received.shape), EP, split_axis=0, concat_a...  7.59 us
    all_to_all x1, starting transfers between devices, shards(): lax.all_to_all(result.reshape(received.shape), EP, split_axis=0, concat_a...  6.15 us
    dot_general x1, matrix products, shards(): jnp.dot(own_hidden, lax.all_gather(d_down, EP, axis=0, tiled=True), prefe...  5.27 us
  transfers between devices with their start and end apart: 7, of which 5 were waited for; matrix products, arithmetic and copies ran while one was open for 12% of the time, Pallas kernels for 0%

commit v1 on v0

--- a/solution.py
+++ b/solution.py
@@ -30,7 +30,9 @@
 def all_blocks(x, axes, sequence):
     tiles = x[None]
     for k in sequence:
-        tiles = lax.all_gather(tiles, axes[k], axis=0, tiled=True)
+        tiles = jnp.concatenate(
+            lax.all_to_all(jnp.stack([tiles] * lax.axis_size(axes[k])), axes[k], 0, 0), axis=0
+        )
     current = [lax.axis_size(axes[k]) for k in reversed(sequence)]
     tiles = tiles.reshape(*current, *x.shape)
     turned = sorted(range(len(sequence)), key=lambda place: sequence[len(sequence) - 1 - place])

time: 222 us -> 236 us (1.063)
  blocking collectives: 65.4 us -> 31.7 us
  waiting for transfers between devices: 65.6 us -> 96.4 us
  starting transfers between devices: 24.6 us -> 33.5 us
  local copies, waits for them, and re-layouts: 14.4 us -> 18.7 us
  other arithmetic: 9.43 us -> 13 us
    all_gather x2 -> x0, blocking collectives: 36.5 us -> none  [all_blocks(): tiles = lax.all_gather(tiles, axes[k], axis=0, tiled=True)]
    all_to_all x0 -> x2, waiting for transfers between devices: none -> 32.9 us  [all_blocks(): lax.all_to_all(jnp.stack([tiles] * lax.axis_size(axes[k])), axes[k], 0, 0)]
    all_to_all x0 -> x2, starting transfers between devices: none -> 9.05 us  [all_blocks(): lax.all_to_all(jnp.stack([tiles] * lax.axis_size(axes[k])), axes[k], 0, 0)]
    all_to_all x0 -> x1, blocking collectives: none -> 6.82 us  [all_blocks(): lax.all_to_all(jnp.stack([tiles] * lax.axis_size(axes[k])), axes[k], 0, 0)]
    all_to_all x1, blocking collectives: 28.8 us -> 24.9 us  [shards(): lax.all_to_all(outbound, EP, split_axis=0, concat_axis=0, tiled=True)]
    another operation x1 -> x3, local copies, waits for them, and re-layouts: 0.11 us -> 2.65 us  [the longest x2 2.55 us: all_blocks(): jnp.stack([tiles] * lax.axis_size(axes[k]))]
  transfers between devices with their start and end apart: 7 -> 8, of which waited for: 5 -> 7; matrix products, arithmetic and copies ran while one was open for 12% -> 22% of each run, Pallas kernels for 0% -> 0%
where the time goes in v1:
time: 236 us; the launch traced here: 235 us
  waiting for transfers between devices  96.4 us (41%)
  starting transfers between devices  33.5 us (14%)
  blocking collectives  31.7 us (13%)
  matrix products  27.1 us (11%)
  local copies, waits for them, and re-layouts  18.7 us (8%)
  between operations  14.4 us (6%)
  other arithmetic  13 us (6%)
    all_to_all x3, waiting for transfers between devices, copy_for_each(): lax.all_to_all(jnp.broadcast_to(x[None], (devices, *x.shape)), axis, 0, 0...  44.4 us
    all_to_all x2, waiting for transfers between devices, all_blocks(): lax.all_to_all(jnp.stack([tiles] * lax.axis_size(axes[k])), axes[k], 0, 0)  32.9 us
    all_to_all x1, blocking collectives, shards(): lax.all_to_all(outbound, EP, split_axis=0, concat_axis=0, tiled=True)  24.9 us
    all_to_all x3, starting transfers between devices, copy_for_each(): lax.all_to_all(jnp.broadcast_to(x[None], (devices, *x.shape)), axis, 0, 0...  13.9 us
    all_to_all x1, waiting for transfers between devices, shards(): lax.all_to_all(dense_hidden, EP, split_axis=0, concat_axis=1, tiled=True)  10.8 us
    all_to_all x2, starting transfers between devices, all_blocks(): lax.all_to_all(jnp.stack([tiles] * lax.axis_size(axes[k])), axes[k], 0, 0)  9.05 us
    all_to_all x1, waiting for transfers between devices, shards(): lax.all_to_all(result.reshape(received.shape), EP, split_axis=0, concat_a...  7.67 us
    all_to_all x1, blocking collectives, all_blocks(): lax.all_to_all(jnp.stack([tiles] * lax.axis_size(axes[k])), axes[k], 0, 0)  6.82 us
  transfers between devices with their start and end apart: 8, of which 7 were waited for; matrix products, arithmetic and copies ran while one was open for 22% of the time, Pallas kernels for 0%

profile of v1, /device:TPU:1, one launch (start us, length us, event | category | flops | bytes accessed | tf_op | source)
XLA Modules:
  0.0 235.0 jit_solution(7203122780323774424)
XLA Ops:
  9.7 2.1 convolution_convert_fusion.5
  15.3 2.6 %convolution_add_fusion = f32[24,8,8,128]{3,2,1,0:T(8,128)} fusion(f32[24,8,8,128]{3,1,2,0:T(8,128)} %get-tuple-element.6, f32[24,8,8]{2,1,0:T(8,128)S(1)} %copy.67), kind=kOutput, calls=%fused_computation.11 | convolution fusion | flops 302202880 | bytes 1579008 | tf_op jit(solution)/shard_map/...ij,jk->...ik/dot_general | solution.py:57
  17.9 2.1 reshape.208
  20.0 3.3 %fusion.10 = bf16[24,8,64]{2,1,0:T(8,128)(2,1)S(1)} fusion(bf16[24,1,1024,64]{2,3,1,0:T(8,128)(2,1)} %param.29, f32[24,8,1024]{2,1,0:T(8,128)} %reshape.208, f32[24,8,1024]{2,1,0:T(8,128)} %copy-done.1, pred[24,1024]{1,0:T(8,128)(4,1)S(1)} %iota_compare_fusion), kind=kOutput, calls=%fused_computation.17 | convolution fusion | flops 27340800 | bytes 4767744 | tf_op jit(solution)/shard_map/bkgs,bksd->bkgd/dot_general | solution.py:73
  23.5 2.0 convolution_convert_fusion.1
  26.3 4.8 %all-to-all-start = ((bf16[4,24,2048]{2,1,0:T(8,128)(2,1)}), bf16[4,24,2048]{2,1,0:T(8,128)(2,1)S(1)}, u32[]{:S(2)}, u32[]{:S(2)}) async-start(bf16[4,24,2048]{2,1,0:T(8,128)(2,1)} %broadcast_in_dim.35), calls=%async_computation | async-start | bytes 786432 | tf_op jit(solution)/shard_map/all_to_all | solution.py:16
  33.4 4.0 %all-to-all-done = bf16[4,24,2048]{2,1,0:T(8,128)(2,1)S(1)} async-done(((bf16[4,24,2048]{2,1,0:T(8,128)(2,1)}), bf16[4,24,2048]{2,1,0:T(8,128)(2,1)S(1)}, u32[]{:S(2)}, u32[]{:S(2)}) %all-to-all-start) | async-done | bytes 393248 | tf_op jit(solution)/shard_map/all_to_all | solution.py:16
  40.7 4.8 %all-to-all-start.4 = ((bf16[4,1,24,512]{3,2,1,0:T(8,128)(2,1)}), bf16[4,1,24,512]{3,2,1,0:T(8,128)(2,1)}, u32[]{:S(2)}, u32[]{:S(2)}) async-start(bf16[4,1,24,512]{3,2,1,0:T(8,128)(2,1)} %stack.9), calls=%async_computation.4 | async-start | bytes 196608 | tf_op jit(solution)/shard_map/all_to_all | solution.py:34
  45.8 4.5 %all-to-all-done.4 = bf16[4,1,24,512]{3,2,1,0:T(8,128)(2,1)} async-done(((bf16[4,1,24,512]{3,2,1,0:T(8,128)(2,1)}), bf16[4,1,24,512]{3,2,1,0:T(8,128)(2,1)}, u32[]{:S(2)}, u32[]{:S(2)}) %all-to-all-start.4) | async-done | bytes 98336 | tf_op jit(solution)/shard_map/all_to_all | solution.py:34
  50.3 24.9 %all_to_all.59 = bf16[64,2,512]{2,1,0:T(2,128)(2,1)S(1)} all-to-all(bf16[64,2,512]{2,1,0:T(2,128)(2,1)S(1)} %reshape.213), channel_id=1, replica_groups=mesh['ep_0'=8,'ep_1'=4,'ep_2'=2,'tp'=4] {'ep_0','ep_1','ep_2'}, dimensions={0} | all-to-all | bytes 262144 | tf_op jit(solution)/shard_map/all_to_all | solution.py:170
  75.2 1.9 stack.10
  77.1 4.2 %all-to-all-start.5 = ((bf16[8,4,24,512]{3,2,1,0:T(8,128)(2,1)}), bf16[8,4,24,512]{3,2,1,0:T(8,128)(2,1)}, u32[]{:S(2)}, u32[]{:S(2)}) async-start(bf16[8,4,24,512]{3,2,1,0:T(8,128)(2,1)} %stack.10), calls=%async_computation.5 | async-start | bytes 1572864 | tf_op jit(solution)/shard_map/all_to_all | solution.py:34
  82.1 1.6 convolution_convert_fusion.2
  83.7 28.4 %all-to-all-done.5 = bf16[8,4,24,512]{3,2,1,0:T(8,128)(2,1)} async-done(((bf16[8,4,24,512]{3,2,1,0:T(8,128)(2,1)}), bf16[8,4,24,512]{3,2,1,0:T(8,128)(2,1)}, u32[]{:S(2)}, u32[]{:S(2)}) %all-to-all-start.5) | async-done | bytes 786464 | tf_op jit(solution)/shard_map/all_to_all | solution.py:34
  112.1 1.5 pad_maximum_fusion
  113.6 6.8 %all_to_all.60 = bf16[2,32,24,512]{3,2,1,0:T(8,128)(2,1)} all-to-all(bf16[2,32,24,512]{3,2,1,0:T(8,128)(2,1)S(1)} %pad_maximum_fusion), channel_id=1, replica_groups=mesh['ep_0'=8,'ep_1'=4,'ep_2'=2,'tp'=4] {'ep_2'}, dimensions={0} | all-to-all | bytes 3145728 | tf_op jit(solution)/shard_map/all_to_all | solution.py:34
  121.5 4.3 %all-to-all-start.2 = ((bf16[4,128,1024]{2,1,0:T(8,128)(2,1)}), bf16[4,128,1024]{2,1,0:T(8,128)(2,1)}, u32[]{:S(2)}, u32[]{:S(2)}) async-start(bf16[4,128,1024]{2,1,0:T(8,128)(2,1)} %broadcast_in_dim.44), calls=%async_computation.2 | async-start | bytes 2097152 | tf_op jit(solution)/shard_map/all_to_all | solution.py:16
  125.8 1.6 copy.70
  128.9 11.8 %all-to-all-done.2 = bf16[4,128,1024]{2,1,0:T(8,128)(2,1)} async-done(((bf16[4,128,1024]{2,1,0:T(8,128)(2,1)}), bf16[4,128,1024]{2,1,0:T(8,128)(2,1)}, u32[]{:S(2)}, u32[]{:S(2)}) %all-to-all-start.2) | async-done | bytes 1048608 | tf_op jit(solution)/shard_map/all_to_all | solution.py:16
  140.7 3.1 %broadcast_in_dim.45 = bf16[4,1536,256]{2,1,0:T(8,128)(2,1)} broadcast(bf16[1536,256]{1,0:T(8,128)(2,1)} %convolution_convert_fusion), dimensions={1,2} | broadcast | bytes 3932160 | tf_op jit(solution)/shard_map/broadcast_in_dim | solution.py:16
  143.8 4.8 %all-to-all-start.7 = ((bf16[4,1536,256]{2,1,0:T(8,128)(2,1)}), bf16[4,1536,256]{2,1,0:T(8,128)(2,1)}, u32[]{:S(2)}, u32[]{:S(2)}) async-start(bf16[4,1536,256]{2,1,0:T(8,128)(2,1)} %broadcast_in_dim.45), calls=%async_computation.7 | async-start | bytes 6291456 | tf_op jit(solution)/shard_map/all_to_all | solution.py:16
  148.8 1.9 fusion.15
  150.6 1.8 fusion.16
  156.4 28.6 %all-to-all-done.7 = bf16[4,1536,256]{2,1,0:T(8,128)(2,1)} async-done(((bf16[4,1536,256]{2,1,0:T(8,128)(2,1)}), bf16[4,1536,256]{2,1,0:T(8,128)(2,1)}, u32[]{:S(2)}, u32[]{:S(2)}) %all-to-all-start.7) | async-done | bytes 3145760 | tf_op jit(solution)/shard_map/all_to_all | solution.py:16
  185.1 6.1 %all-to-all-start.3 = ((bf16[64,2,512]{2,1,0:T(2,128)(2,1)}), bf16[64,2,512]{2,1,0:T(2,128)(2,1)S(1)}, u32[]{:S(2)}, u32[]{:S(2)}) async-start(bf16[64,2,512]{2,1,0:T(2,128)(2,1)} %reshape.215), calls=%async_computation.3 | async-start | bytes 262144 | tf_op jit(solution)/shard_map/all_to_all | solution.py:179
  191.2 2.5 %convert_reduce_fusion = f32[1536,256]{1,0:T(8,128)S(1)} fusion(bf16[4,1536,256]{2,1,0:T(8,128)(2,1)} %all-to-all-done.7), kind=kLoop, calls=%fused_computation | loop fusion | flops 2752512 | bytes 4718592 | tf_op jit(solution)/shard_map/reduce_sum | solution.py:21
  194.8 7.7 %all-to-all-done.3 = bf16[64,2,512]{2,1,0:T(2,128)(2,1)S(1)} async-done(((bf16[64,2,512]{2,1,0:T(2,128)(2,1)}), bf16[64,2,512]{2,1,0:T(2,128)(2,1)S(1)}, u32[]{:S(2)}, u32[]{:S(2)}) %all-to-all-start.3) | async-done | bytes 131104 | tf_op jit(solution)/shard_map/all_to_all | solution.py:179
  203.1 4.5 %all-to-all-start.8 = ((bf16[64,24,128]{2,1,0:T(8,128)(2,1)}), bf16[64,24,128]{2,1,0:T(8,128)(2,1)S(1)}, u32[]{:S(2)}, u32[]{:S(2)}) async-start(bf16[64,24,128]{2,1,0:T(8,128)(2,1)} %bitcast.85), calls=%async_computation.8 | async-start | bytes 786432 | tf_op jit(solution)/shard_map/all_to_all | solution.py:196
  208.6 1.7 reshape.221
  210.3 1.8 convolution_reduce_fusion
  212.1 10.8 %all-to-all-done.8 = bf16[64,24,128]{2,1,0:T(8,128)(2,1)S(1)} async-done(((bf16[64,24,128]{2,1,0:T(8,128)(2,1)}), bf16[64,24,128]{2,1,0:T(8,128)(2,1)S(1)}, u32[]{:S(2)}, u32[]{:S(2)}) %all-to-all-start.8) | async-done | bytes 393248 | tf_op jit(solution)/shard_map/all_to_all | solution.py:196
  222.9 5.3 %fusion.14 = bf16[24,512]{1,0:T(8,128)(2,1)} fusion(bf16[8192,512]{1,0:T(8,128)(2,1)} %all-gather.2.cloned.1.call-done, f32[24,512]{1,0:T(8,128)} %convolution_reduce_fusion, f32[24,2048]{1,0:T(8,128)} %copy-done.2, s32[]{:T(128)S(6)} %select_n.41, f32[24]{0:T(128)S(1)} %fusion.20, bf16[64,24,128]{2,1,0:T(8,128)(2,1)S(1)} %all-to-all-done.8), kind=kOutput, calls=%fused_computation.21 | convolution fusion | flops 201375744 | bytes 8904804 | tf_op jit(solution)/shard_map/dot_general | solution.py:197
  (83 shorter events, 22.8 us)
Async XLA Ops:
  7.2 4.8 %copy-start = (bf16[24,1,1024,64]{2,3,1,0:T(8,128)(2,1)S(1)}, bf16[24,1,1024,64]{2,3,1,0:T(8,128)(2,1)}, u32[]{:S(2)}) copy-start(bf16[24,1,1024,64]{2,3,1,0:T(8,128)(2,1)} %param.28) | copy-start | bytes 9437188
  7.2 4.7 %copy-start.11 = (s32[24]{0:T(128)S(1)}, s32[24]{0:T(128)}, u32[]{:S(2)}) copy-start(s32[24]{0:T(128)} %param.30) | copy-start | bytes 292
  7.2 4.8 %copy-start.8 = (f32[8]{0:T(128)S(1)}, f32[8]{0:T(128)}, u32[]{:S(2)}) copy-start(f32[8]{0:T(128)} %param.27) | copy-start | bytes 100
  7.2 215.7 %all-gather.2.cloned.1.call-start = ((), (), s32[]{:S(2)}) async-start(), calls=%async_computation.9 | async-start | bytes 8519680 | tf_op jit(solution)/shard_map/all_gather | solution.py:199
  9.2 0.5 copy-start.9
  12.5 0.9 copy-start.1
  23.3 7.8 %copy-start.6 = (s32[24,2]{0,1:T(2,128)S(1)}, s32[24,2]{0,1:T(2,128)}, u32[]{:S(2)}) copy-start(s32[24,2]{0,1:T(2,128)} %param.34) | copy-start | bytes 580
  26.3 11.1 %all-to-all-start = ((bf16[4,24,2048]{2,1,0:T(8,128)(2,1)}), bf16[4,24,2048]{2,1,0:T(8,128)(2,1)S(1)}, u32[]{:S(2)}, u32[]{:S(2)}) async-start(bf16[4,24,2048]{2,1,0:T(8,128)(2,1)} %broadcast_in_dim.35), calls=%async_computation | async-start | bytes 786432 | tf_op jit(solution)/shard_map/all_to_all | solution.py:16
  32.7 4.7 %copy-start.12 = (s32[48]{0:T(128)}, s32[48]{0:T(128)S(1)}, u32[]{:S(2)}) copy-start(s32[48]{0:T(128)S(1)} %convert_reduce_fusion.3) | copy-start | bytes 580
  38.5 0.7 copy-start.2
  40.0 112.7 %copy-start.5 = (bf16[24,2048]{1,0:T(8,128)(2,1)}, bf16[24,2048]{1,0:T(8,128)(2,1)S(1)}, u32[]{:S(2)}) copy-start(bf16[24,2048]{1,0:T(8,128)(2,1)S(1)} %multiply_convert_fusion) | copy-start | bytes 294916
  40.7 9.6 %all-to-all-start.4 = ((bf16[4,1,24,512]{3,2,1,0:T(8,128)(2,1)}), bf16[4,1,24,512]{3,2,1,0:T(8,128)(2,1)}, u32[]{:S(2)}, u32[]{:S(2)}) async-start(bf16[4,1,24,512]{3,2,1,0:T(8,128)(2,1)} %stack.9), calls=%async_computation.4 | async-start | bytes 196608 | tf_op jit(solution)/shard_map/all_to_all | solution.py:34
  77.1 34.9 %all-to-all-start.5 = ((bf16[8,4,24,512]{3,2,1,0:T(8,128)(2,1)}), bf16[8,4,24,512]{3,2,1,0:T(8,128)(2,1)}, u32[]{:S(2)}, u32[]{:S(2)}) async-start(bf16[8,4,24,512]{3,2,1,0:T(8,128)(2,1)} %stack.10), calls=%async_computation.5 | async-start | bytes 1572864 | tf_op jit(solution)/shard_map/all_to_all | solution.py:34
  121.5 19.1 %all-to-all-start.2 = ((bf16[4,128,1024]{2,1,0:T(8,128)(2,1)}), bf16[4,128,1024]{2,1,0:T(8,128)(2,1)}, u32[]{:S(2)}, u32[]{:S(2)}) async-start(bf16[4,128,1024]{2,1,0:T(8,128)(2,1)} %broadcast_in_dim.44), calls=%async_computation.2 | async-start | bytes 2097152 | tf_op jit(solution)/shard_map/all_to_all | solution.py:16
  125.8 1.7 copy-start.15
  125.8 1.7 copy-start.16
  143.8 4.8 %copy-start.13 = (s32[48]{0:T(128)S(1)}, s32[48]{0:T(128)}, u32[]{:S(2)}) copy-start(s32[48]{0:T(128)} %copy-done.12) | copy-start | bytes 580
  143.8 5.0 %copy-start.3 = (bf16[24,2048]{1,0:T(8,128)(2,1)S(1)}, bf16[24,2048]{1,0:T(8,128)(2,1)}, u32[]{:S(2)}) copy-start(bf16[24,2048]{1,0:T(8,128)(2,1)} %param.21) | copy-start | bytes 294916
  143.8 5.0 %copy-start.7 = (f32[2048]{0:T(1024)S(1)}, f32[2048]{0:T(1024)}, u32[]{:S(2)}) copy-start(f32[2048]{0:T(1024)} %param.22) | copy-start | bytes 24580
  143.8 5.0 %copy-start.10 = (f32[24]{0:T(128)S(1)}, f32[24]{0:T(128)}, u32[]{:S(2)}) copy-start(f32[24]{0:T(128)} %copy-done.9) | copy-start | bytes 292
  143.8 8.7 %copy-start.17 = (bf16[2048,4]{0,1:T(4,128)(2,1)S(1)}, bf16[2048,4]{0,1:T(4,128)(2,1)}, u32[]{:S(2)}) copy-start(bf16[2048,4]{0,1:T(4,128)(2,1)} %param.32) | copy-start | bytes 49156
  143.8 41.3 %all-to-all-start.7 = ((bf16[4,1536,256]{2,1,0:T(8,128)(2,1)}), bf16[4,1536,256]{2,1,0:T(8,128)(2,1)}, u32[]{:S(2)}, u32[]{:S(2)}) async-start(bf16[4,1536,256]{2,1,0:T(8,128)(2,1)} %broadcast_in_dim.45), calls=%async_computation.7 | async-start | bytes 6291456 | tf_op jit(solution)/shard_map/all_to_all | solution.py:16
  148.8 6.7 %copy-start.14 = (bf16[1,512,512]{2,1,0:T(8,128)(2,1)S(1)}, bf16[1,512,512]{2,1,0:T(8,128)(2,1)}, u32[]{:S(2)}) copy-start(bf16[1,512,512]{2,1,0:T(8,128)(2,1)} %param.37) | copy-start | bytes 1572868
  185.1 17.4 %all-to-all-start.3 = ((bf16[64,2,512]{2,1,0:T(2,128)(2,1)}), bf16[64,2,512]{2,1,0:T(2,128)(2,1)S(1)}, u32[]{:S(2)}, u32[]{:S(2)}) async-start(bf16[64,2,512]{2,1,0:T(2,128)(2,1)} %reshape.215), calls=%async_computation.3 | async-start | bytes 262144 | tf_op jit(solution)/shard_map/all_to_all | solution.py:179
  202.4 0.7 copy-start.4
  203.1 19.8 %all-to-all-start.8 = ((bf16[64,24,128]{2,1,0:T(8,128)(2,1)}), bf16[64,24,128]{2,1,0:T(8,128)(2,1)S(1)}, u32[]{:S(2)}, u32[]{:S(2)}) async-start(bf16[64,24,128]{2,1,0:T(8,128)(2,1)} %bitcast.85), calls=%async_computation.8 | async-start | bytes 786432 | tf_op jit(solution)/shard_map/all_to_all | solution.py:196
Sparse Core Ops, SparseCore 0:
  10.8 100.6 all-gather.1
